TPU v7x, 32 devices: a whole 2x2x4 slice. The times are simulated.
32 devices in a mesh: sp: 8 (over z, x), tp: 4 (over y, core).
Axes of the slice: x: 2, y: 2, z: 4, core: 2. Of those that a mesh axis runs over, the one named last changes fastest.
Arguments:
- tokens: bfloat16 [1536, 2048], P(('sp', 'tp')), may hold values from -54 to 54
- w_query: bfloat16 [2048, 2048], P(None, 'tp'), may hold values from -0.21875 to 0.21875
- w_key: bfloat16 [2048, 2048], P(None, 'tp'), may hold values from -0.125 to 0.125
- w_value: bfloat16 [2048, 2048], P(None, 'tp'), may hold values from -0.125 to 0.125
- w_out: bfloat16 [2048, 2048], P('tp'), may hold values from -0.125 to 0.125
- mix_weight: float32 [16], P('tp'), may hold values from 0.3 to 0.8
- out_gain: float32 [128], replicated, may hold values from 0.1 to 1.9
Outputs:
- mixed: bfloat16 [1536, 2048], P(('sp', 'tp'))
All inputs are finite; a program needn't handle non-finite values.
Results may differ from a plain program's by a relative error of at most 0.018.
The roundings to bfloat16 on the way count: a program that leaves them out, or rounds other values in their place, can miss the bound.
Values may be sent and summed in bfloat16 or wider, within the bound.
No kernel may reach another device: no remote copies, remote signals or barrier semaphores. Data moves between devices by JAX's collectives and lax.ppermute only.
A program may use at most 192 MiB of HBM per device.

v0:
```python
import jax
import jax.numpy as jnp
from jax import lax
from jax.experimental import pallas as pl
from jax.experimental.pallas import tpu as pltpu
from jax.sharding import PartitionSpec as P


VMEM = pl.BlockSpec(memory_space=pltpu.VMEM)
SMEM = pl.BlockSpec(memory_space=pltpu.SMEM)
F32 = jnp.float32
BF16 = jnp.bfloat16
LOG2E = 1.4426950408889634


def swap(array, axis, size, mask):
    return lax.ppermute(array, axis, [(i, i ^ mask) for i in range(size)])


def project_own(x, weights):
    rows = x.shape[0]

    def body(x_ref, *refs):
        for w, o in zip(refs[:3], refs[3:]):
            o[...] = jnp.dot(x_ref[...], w[...], preferred_element_type=F32).astype(BF16)

    flops = sum(2 * rows * w.size for w in weights)
    return pl.pallas_call(
        body,
        out_shape=[jax.ShapeDtypeStruct((rows, w.shape[1]), BF16) for w in weights],
        in_specs=[VMEM] * 4,
        out_specs=[VMEM] * 3,
        cost_estimate=pl.CostEstimate(
            flops=8 * flops, bytes_accessed=sum(2 * w.size for w in weights), transcendentals=0
        ),
        compiler_params=pltpu.CompilerParams(vmem_limit_bytes=12 << 20),
        name="project_own",
    )(x, *weights)


def project(own, blocks, weights, heads, sharing):
    start = own[0].shape[0]
    rows = start + sum(b.shape[0] for b in blocks)
    widths = [w.shape[1] // heads for w in weights]
    n = len(blocks)

    def body(*refs):
        own_head = lax.axis_index("sp") // sharing
        firsts, ins, ws = refs[:3], refs[3 : n + 3], refs[n + 3 : n + 6]
        outs, res = refs[n + 6 : -3], refs[-3:]
        if n:
            x = jnp.concatenate([r[...] for r in ins], axis=0)
        at = 0
        for i, (f, w, s, width) in enumerate(zip(firsts, ws, res, widths)):
            s[:start, :] = f[...]
            if n:
                s[start:, :] = jnp.dot(x, w[...], preferred_element_type=F32).astype(BF16)
            for j in range(heads):
                h = own_head ^ j
                part = s[:, pl.ds(pl.multiple_of(h * width, width), width)]
                outs[j][:, at : at + width] = part
                if sharing > 1 and i < 2:
                    outs[heads + j][:, at : at + width] = part
            at += width

    shapes = [jax.ShapeDtypeStruct((rows, sum(widths)), BF16)] * heads
    if sharing > 1:
        shapes += [jax.ShapeDtypeStruct((rows, sum(widths[:2])), BF16)] * heads
    return pl.pallas_call(
        body,
        out_shape=shapes,
        in_specs=[VMEM] * (n + 6),
        out_specs=[VMEM] * len(shapes),
        scratch_shapes=[pltpu.VMEM((rows, w.shape[1]), BF16) for w in weights],
        compiler_params=pltpu.CompilerParams(vmem_limit_bytes=20 << 20),
        name="project",
    )(*own, *blocks, *weights)


def attend(q_parts, kv_parts, mix, gain, sharing, qk, vd):
    nq = len(q_parts)
    rows = q_parts[0].shape[0]
    parts = list(q_parts) + list(kv_parts)
    n = len(parts)
    queries, keys = nq * rows, n * rows
    half = qk // 2
    block = 256 if queries % 256 == 0 else rows
    chunk = max(c * rows for c in range(1, n + 1) if n % c == 0 and c * rows <= 2048)
    factor = half**-0.5 * LOG2E

    def body(mix_ref, gain_ref, *refs):
        own_head = lax.axis_index("sp") // sharing
        ins, outs, (sk, sv, sq, so) = refs[:n], refs[n : n + nq], refs[n + nq :]
        for i, r in enumerate(ins):
            at = i * rows
            sk[at : at + rows, :] = r[:, :qk]
            c, o = divmod(at, chunk)
            sv[c, :, o : o + rows] = r[:, qk : qk + vd].astype(F32).T.astype(BF16)
            if i < nq:
                sq[at : at + rows, :] = r[:, qk + vd :]
        lam = mix_ref[own_head]
        lane = lax.broadcasted_iota(jnp.int32, (block, qk), 1)

        def piece(q, c):
            at = c * chunk if isinstance(c, int) else pl.multiple_of(c * chunk, rows)
            s = lax.dot_general(
                sk[pl.ds(at, chunk), :], q, (((1,), (1,)), ((), ())), preferred_element_type=F32
            )
            return s, jnp.max(s, axis=0, keepdims=True)

        def softmax(q):
            if keys == chunk:
                s, top = piece(q, 0)
                e = jnp.exp2((s - top) * factor)
                acc = jnp.dot(sv[0], e.astype(BF16), preferred_element_type=F32)
                return acc / jnp.sum(e, axis=0, keepdims=True)

            def step(c, carry):
                old, total, acc = carry
                s, top = piece(q, c)
                top = jnp.maximum(old, top)
                fix = jnp.exp2((old - top) * factor)
                e = jnp.exp2((s - top) * factor)
                acc = acc * fix + jnp.dot(sv[c], e.astype(BF16), preferred_element_type=F32)
                return top, total * fix + jnp.sum(e, axis=0, keepdims=True), acc

            start = (
                jnp.full((1, block), -1e30, F32),
                jnp.zeros((1, block), F32),
                jnp.zeros((vd, block), F32),
            )
            top, total, acc = lax.fori_loop(0, keys // chunk, step, start)
            return acc / total

        for b in range(queries // block):
            q = sq[b * block : (b + 1) * block, :]
            zero = jnp.zeros_like(q)
            first = softmax(jnp.where(lane < half, q, zero))
            second = softmax(jnp.where(lane < half, zero, q))
            ho = first - lam * second
            ho = ho * lax.rsqrt(jnp.mean(ho * ho, axis=0, keepdims=True) + 1e-06)
            so[b * block : (b + 1) * block, :] = (ho.T * gain_ref[...]).astype(BF16)
        for i in range(nq):
            outs[i][...] = so[i * rows : (i + 1) * rows, :]

    return pl.pallas_call(
        body,
        out_shape=[jax.ShapeDtypeStruct((rows, vd), BF16)] * nq,
        in_specs=[SMEM] + [VMEM] * (n + 1),
        out_specs=[VMEM] * nq,
        scratch_shapes=[
            pltpu.VMEM((keys, qk), BF16),
            pltpu.VMEM((keys // chunk, vd, chunk), BF16),
            pltpu.VMEM((queries, qk), BF16),
            pltpu.VMEM((queries, vd), BF16),
        ],
        compiler_params=pltpu.CompilerParams(vmem_limit_bytes=24 << 20),
        name="attend",
    )(mix, gain.reshape(1, vd), *parts)


def project_out(normed, w_out, sharing, masks, rows):
    heads = len(normed)
    total, vd = normed[0].shape

    def body(*refs):
        own_head = lax.axis_index("sp") // sharing
        ins, w, outs, sx = refs[:heads], refs[heads], refs[heads + 1 : -1], refs[-1]
        for j in range(heads):
            h = own_head ^ j
            sx[:, pl.ds(pl.multiple_of(h * vd, vd), vd)] = ins[j][...]
        y = jnp.dot(sx[...], w[...], preferred_element_type=F32)
        for i in range(len(masks)):
            outs[i][...] = y[i * rows : (i + 1) * rows].astype(BF16)

    return pl.pallas_call(
        body,
        out_shape=[jax.ShapeDtypeStruct((rows, w_out.shape[1]), BF16)] * len(masks),
        in_specs=[VMEM] * (heads + 1),
        out_specs=[VMEM] * len(masks),
        scratch_shapes=[pltpu.VMEM((total, heads * vd), BF16)],
        compiler_params=pltpu.CompilerParams(vmem_limit_bytes=12 << 20),
        name="project_out",
    )(*normed, w_out)


def make(n_sp, n_tp):
    def shards(tokens, w_query, w_key, w_value, w_out, mix_weight, out_gain):
        heads = mix_weight.shape[0]
        qk = w_query.shape[1] // heads
        vd = w_value.shape[1] // heads
        rows = tokens.shape[0]
        sharing = n_sp // heads

        weights = (w_key, w_value, w_query)
        bits = []
        while (1 << len(bits)) < n_tp:
            bits.append(1 << len(bits))
        masks, blocks = [0], [tokens]
        for bit in reversed(bits):
            blocks = blocks + [swap(b, "tp", n_tp, bit) for b in blocks]
            masks = masks + [m | bit for m in masks]

        own = project_own(tokens, weights)
        mine = project(own, blocks[1:], weights, heads, sharing)
        q_parts = [mine[0]] + [None] * (heads - 1)
        kv_parts = {}
        relay = heads // 2
        order = ([relay] if relay else []) + [j for j in reversed(range(heads)) if j != relay]
        for j in order:
            if j:
                q_parts[j] = swap(mine[j], "sp", n_sp, j * sharing)
            if not (j and j == relay):
                for r in range(1, sharing):
                    kv_parts[j, r] = swap(mine[heads + j], "sp", n_sp, j * sharing + r)
        if relay:
            for r in range(1, sharing):
                kv_parts[relay, r] = swap(q_parts[relay], "sp", n_sp, r)
        kv_parts = list(kv_parts.values())
        out = attend(q_parts, kv_parts, mix_weight, out_gain, sharing, qk, vd)
        normed = [out[0]] + [swap(out[j], "sp", n_sp, j * sharing) for j in range(1, heads)]
        parts = dict(zip(masks, project_out(normed, w_out, sharing, masks, rows)))
        for bit in bits:
            moved = {m: swap(p, "tp", n_tp, bit) for m, p in parts.items() if m & bit}
            parts = {
                m: (p.astype(F32) + moved[m | bit].astype(F32)).astype(BF16)
                for m, p in parts.items()
                if not m & bit
            }
        return parts[0]

    return shards


def solution(mesh):
    in_specs = (
        P(("sp", "tp"), None),
        P(None, "tp"),
        P(None, "tp"),
        P(None, "tp"),
        P("tp", None),
        P("tp"),
        P(),
    )
    out_specs = P(("sp", "tp"), None)
    inner = make(mesh.shape["sp"], mesh.shape["tp"])

    return jax.shard_map(inner, mesh=mesh, in_specs=in_specs, out_specs=out_specs, check_vma=False)
```

profile of v0, /device:TPU:0, one launch (start us, length us, event | category | flops | bytes accessed | tf_op | source)
XLA Modules:
  0.0 68.7 jit_solution(6479977932114197066)
XLA Ops:
  0.0 3.0 %collective-permute-start = (bf16[48,2048]{1,0:T(8,128)(2,1)}, bf16[48,2048]{1,0:T(8,128)(2,1)S(1)}, u32[]{:S(2)}, u32[]{:S(2)}) collective-permute-start(bf16[48,2048]{1,0:T(8,128)(2,1)} %x_ref.1), channel_id=1, source_target_pairs={{0,2},{1,3},{2,0},{3,1},{4,6},{5,7},{6,4},{7,5},{8,10},{9,11},{10,... | collective-permute-start | bytes 589832 | tf_op jit(solution)/shard_map/ppermute | solution.py:17
  3.0 0.0 collective-permute-start.1
  3.0 5.1 %collective-permute-done.refs_3_ = bf16[48,2048]{1,0:T(8,128)(2,1)S(1)} collective-permute-done((bf16[48,2048]{1,0:T(8,128)(2,1)}, bf16[48,2048]{1,0:T(8,128)(2,1)S(1)}, u32[]{:S(2)}, u32[]{:S(2)}) %collective-permute-start) | collective-permute-done | bytes 196640 | tf_op jit(solution)/shard_map/ppermute | solution.py:17
  8.1 0.0 collective-permute-start.2
  8.1 0.0 copy-start
  8.1 1.6 %copy-done = bf16[2048,512]{1,0:T(8,128)(2,1)S(1)} copy-done((bf16[2048,512]{1,0:T(8,128)(2,1)S(1)}, bf16[2048,512]{1,0:T(8,128)(2,1)}, u32[]{:S(2)}) %copy-start) | copy-done | bytes 2097176
  9.7 0.0 copy-start.2
  9.7 1.6 %copy-done.2 = bf16[2048,512]{1,0:T(8,128)(2,1)S(1)} copy-done((bf16[2048,512]{1,0:T(8,128)(2,1)S(1)}, bf16[2048,512]{1,0:T(8,128)(2,1)}, u32[]{:S(2)}) %copy-start.2) | copy-done | bytes 2097176
  11.3 0.0 copy-start.4
  11.3 1.6 %copy-done.4 = bf16[2048,512]{1,0:T(8,128)(2,1)S(1)} copy-done((bf16[2048,512]{1,0:T(8,128)(2,1)S(1)}, bf16[2048,512]{1,0:T(8,128)(2,1)}, u32[]{:S(2)}) %copy-start.4) | copy-done | bytes 2097176
  12.9 0.0 copy-start.9
  12.9 0.9 %copy-done.9 = bf16[48,2048]{1,0:T(8,128)(2,1)S(1)} copy-done((bf16[48,2048]{1,0:T(8,128)(2,1)S(1)}, bf16[48,2048]{1,0:T(8,128)(2,1)}, u32[]{:S(2)}) %copy-start.9) | copy-done | bytes 196632
  13.8 0.0 copy-start.1
  13.8 0.0 copy-start.3
  13.8 0.0 copy-start.5
  13.8 1.2 %project_own.1 = (bf16[48,512]{1,0:T(8,128)(2,1)S(1)}, bf16[48,512]{1,0:T(8,128)(2,1)S(1)}, bf16[48,512]{1,0:T(8,128)(2,1)S(1)}) custom-call(bf16[48,2048]{1,0:T(8,128)(2,1)S(1)} %copy-done.9, bf16[2048,512]{1,0:T(8,128)(2,1)S(1)} %copy-done, bf16[2048,512]{1,0:T(8,128)(2,1)S(1)} %copy-done.2, bf16[2048,512]{1,0:T(8,128)(2,1)S(1)} %copy-done.4), custom_call_target="tpu_custom_call" | custom-call | flops 2415919104 | bytes 6291456 | tf_op jit(solution)/shard_map/project_own/pallas_call | solution.py:28
  15.0 0.0 collective-permute-done.1.refs_4_
  15.0 0.0 collective-permute-done.2.refs_5_
  15.0 0.4 copy-done.1
  15.4 0.6 copy-done.3
  16.0 0.6 copy-done.5
  16.7 0.0 copy-start.7
  16.7 0.0 copy-start.8
  16.7 0.0 copy-start.6
  16.7 1.7 %project.1 = (bf16[192,384]{1,0:T(8,128)(2,1)S(1)}, bf16[192,384]{1,0:T(8,128)(2,1)S(1)}, bf16[192,384]{1,0:T(8,128)(2,1)S(1)}, bf16[192,384]{1,0:T(8,128)(2,1)S...) custom-call(bf16[48,512]{1,0:T(8,128)(2,1)S(1)} %get-tuple-element.2, ...), custom_call_target="tpu_custom_call" | custom-call | tf_op jit(solution)/shard_map/project/pallas_call | solution.py:69
  18.3 2.8 %collective-permute-start.4 = (bf16[192,384]{1,0:T(8,128)(2,1)S(1)}, bf16[192,384]{1,0:T(8,128)(2,1)S(1)}, u32[]{:S(2)}, u32[]{:S(2)}) collective-permute-start(bf16[192,384]{1,0:T(8,128)(2,1)S(1)} %get-tuple-element.28), channel_id=1, source_target_pairs={{0,16},{4,20},{8,24},{12,28},{16,0},{20,4},{24,8},{28,12},{1,17},{... | collective-permute-start | bytes 442376 | tf_op jit(solution)/shard_map/ppermute | solution.py:17
  21.1 2.3 %collective-permute-start.6 = (bf16[192,256]{1,0:T(8,128)(2,1)S(1)}, bf16[192,256]{1,0:T(8,128)(2,1)S(1)}, u32[]{:S(2)}, u32[]{:S(2)}) collective-permute-start(bf16[192,256]{1,0:T(8,128)(2,1)S(1)} %get-tuple-element.30), channel_id=1, source_target_pairs={{0,28},{4,24},{8,20},{12,16},{16,12},{20,8},{24,4},{28,0},{1,29},{... | collective-permute-start | bytes 294920 | tf_op jit(solution)/shard_map/ppermute | solution.py:17
  23.4 0.0 collective-permute-start.3
  23.4 3.2 %collective-permute-start.5 = (bf16[192,384]{1,0:T(8,128)(2,1)S(1)}, bf16[192,384]{1,0:T(8,128)(2,1)S(1)}, u32[]{:S(2)}, u32[]{:S(2)}) collective-permute-start(bf16[192,384]{1,0:T(8,128)(2,1)S(1)} %get-tuple-element.29), channel_id=1, source_target_pairs={{0,24},{4,28},{8,16},{12,20},{16,8},{20,12},{24,0},{28,4},{1,25},{... | collective-permute-start | bytes 442376 | tf_op jit(solution)/shard_map/ppermute | solution.py:17
  26.6 4.7 %collective-permute-done.4.refs_2_ = bf16[192,384]{1,0:T(8,128)(2,1)S(1)} collective-permute-done((bf16[192,384]{1,0:T(8,128)(2,1)S(1)}, bf16[192,384]{1,0:T(8,128)(2,1)S(1)}, u32[]{:S(2)}, u32[]{:S(2)}) %collective-permute-start.4) | collective-permute-done | bytes 147488 | tf_op jit(solution)/shard_map/ppermute | solution.py:17
  31.3 1.7 %collective-permute-start.9 = (bf16[192,384]{1,0:T(8,128)(2,1)S(1)}, bf16[192,384]{1,0:T(8,128)(2,1)S(1)}, u32[]{:S(2)}, u32[]{:S(2)}) collective-permute-start(bf16[192,384]{1,0:T(8,128)(2,1)S(1)} %collective-permute-done.4.refs_2_), channel_id=1, source_target_pairs={{0,4},{4,0},{8,12},{12,8},{16,20},{20,16},{24,28},{28,24},{1,5},{5... | collective-permute-start | bytes 442376 | tf_op jit(solution)/shard_map/ppermute | solution.py:17
  33.0 0.5 collective-permute-start.7
  33.5 0.0 collective-permute-done.6.refs_4_
  33.5 1.5 %collective-permute-start.8 = (bf16[192,256]{1,0:T(8,128)(2,1)S(1)}, bf16[192,256]{1,0:T(8,128)(2,1)S(1)}, u32[]{:S(2)}, u32[]{:S(2)}) collective-permute-start(bf16[192,256]{1,0:T(8,128)(2,1)S(1)} %get-tuple-element.32), channel_id=1, source_target_pairs={{0,4},{4,0},{8,12},{12,8},{16,20},{20,16},{24,28},{28,24},{1,5},{5... | collective-permute-start | bytes 294920 | tf_op jit(solution)/shard_map/ppermute | solution.py:17
  35.0 3.6 %collective-permute-done.7.refs_5_ = bf16[192,256]{1,0:T(8,128)(2,1)S(1)} collective-permute-done((bf16[192,256]{1,0:T(8,128)(2,1)S(1)}, bf16[192,256]{1,0:T(8,128)(2,1)S(1)}, u32[]{:S(2)}, u32[]{:S(2)}) %collective-permute-start.7) | collective-permute-done | bytes 98336 | tf_op jit(solution)/shard_map/ppermute | solution.py:17
  38.6 2.1 %collective-permute-done.8.refs_6_ = bf16[192,256]{1,0:T(8,128)(2,1)S(1)} collective-permute-done((bf16[192,256]{1,0:T(8,128)(2,1)S(1)}, bf16[192,256]{1,0:T(8,128)(2,1)S(1)}, u32[]{:S(2)}, u32[]{:S(2)}) %collective-permute-start.8) | collective-permute-done | bytes 98336 | tf_op jit(solution)/shard_map/ppermute | solution.py:17
  40.8 0.0 collective-permute-done.3.refs_1_
  40.8 0.0 collective-permute-done.5.refs_3_
  40.8 0.0 collective-permute-done.9.refs_7_
  40.8 0.0 copy-done.7
  40.8 0.0 copy-done.8
  40.8 6.3 %attend.1 = (bf16[192,128]{1,0:T(8,128)(2,1)S(1)}, bf16[192,128]{1,0:T(8,128)(2,1)S(1)}, bf16[192,128]{1,0:T(8,128)(2,1)S(1)}, bf16[192,128]{1,0:T(8,128)(2,1)S(1)}) custom-call(f32[4]{0:T(128)S(1)} %copy-done.7, f32[1,128]{1,0:T(1,128)S(1)} %bitcast.1, bf16[192,384]{1,0:T(8,128)(2,1)S(1)} %get-tuple-element.26.refs_0_, ...), custom_call_target="tpu_custom_call" | custom-call | tf_op jit(solution)/shard_map/attend/pallas_call | solution.py:146
  47.1 2.9 %collective-permute-start.10 = (bf16[192,128]{1,0:T(8,128)(2,1)S(1)}, bf16[192,128]{1,0:T(8,128)(2,1)S(1)}, u32[]{:S(2)}, u32[]{:S(2)}) collective-permute-start(bf16[192,128]{1,0:T(8,128)(2,1)S(1)} %get-tuple-element.34), channel_id=1, source_target_pairs={{0,8},{4,12},{8,0},{12,4},{16,24},{20,28},{24,16},{28,20},{1,9},{5... | collective-permute-start | bytes 147464 | tf_op jit(solution)/shard_map/ppermute | solution.py:17
  50.0 2.7 %collective-permute-start.11 = (bf16[192,128]{1,0:T(8,128)(2,1)S(1)}, bf16[192,128]{1,0:T(8,128)(2,1)S(1)}, u32[]{:S(2)}, u32[]{:S(2)}) collective-permute-start(bf16[192,128]{1,0:T(8,128)(2,1)S(1)} %get-tuple-element.35), channel_id=1, source_target_pairs={{0,16},{4,20},{8,24},{12,28},{16,0},{20,4},{24,8},{28,12},{1,17},{... | collective-permute-start | bytes 147464 | tf_op jit(solution)/shard_map/ppermute | solution.py:17
  52.7 1.4 %collective-permute-start.12 = (bf16[192,128]{1,0:T(8,128)(2,1)S(1)}, bf16[192,128]{1,0:T(8,128)(2,1)S(1)}, u32[]{:S(2)}, u32[]{:S(2)}) collective-permute-start(bf16[192,128]{1,0:T(8,128)(2,1)S(1)} %get-tuple-element.36), channel_id=1, source_target_pairs={{0,24},{4,28},{8,16},{12,20},{16,8},{20,12},{24,0},{28,4},{1,25},{... | collective-permute-start | bytes 147464 | tf_op jit(solution)/shard_map/ppermute | solution.py:17
  54.1 0.0 collective-permute-done.10.refs_1_
  54.1 1.1 %collective-permute-done.11.refs_2_ = bf16[192,128]{1,0:T(8,128)(2,1)S(1)} collective-permute-done((bf16[192,128]{1,0:T(8,128)(2,1)S(1)}, bf16[192,128]{1,0:T(8,128)(2,1)S(1)}, u32[]{:S(2)}, u32[]{:S(2)}) %collective-permute-start.11) | collective-permute-done | bytes 49184 | tf_op jit(solution)/shard_map/ppermute | solution.py:17
  55.3 3.5 %collective-permute-done.12.refs_3_ = bf16[192,128]{1,0:T(8,128)(2,1)S(1)} collective-permute-done((bf16[192,128]{1,0:T(8,128)(2,1)S(1)}, bf16[192,128]{1,0:T(8,128)(2,1)S(1)}, u32[]{:S(2)}, u32[]{:S(2)}) %collective-permute-start.12) | collective-permute-done | bytes 49184 | tf_op jit(solution)/shard_map/ppermute | solution.py:17
  58.7 0.0 copy-done.6
  58.7 0.6 project_out.1
  59.4 0.1 collective-permute-start.14
  59.4 0.5 collective-permute-start.13
  59.9 0.9 %collective-permute-done.14 = bf16[48,2048]{1,0:T(8,128)(2,1)S(1)} collective-permute-done((bf16[48,2048]{1,0:T(8,128)(2,1)S(1)}, bf16[48,2048]{1,0:T(8,128)(2,1)S(1)}, u32[]{:S(2)}, u32[]{:S(2)}) %collective-permute-start.14) | collective-permute-done | bytes 196640 | tf_op jit(solution)/shard_map/ppermute | solution.py:17
  60.9 0.1 add_convert_fusion.1
  60.9 1.6 %collective-permute-start.15 = (bf16[48,2048]{1,0:T(8,128)(2,1)S(1)}, bf16[48,2048]{1,0:T(8,128)(2,1)S(1)}, u32[]{:S(2)}, u32[]{:S(2)}) collective-permute-start(bf16[48,2048]{1,0:T(8,128)(2,1)S(1)} %add_convert_fusion.1), channel_id=1, source_target_pairs={{0,2},{1,3},{2,0},{3,1},{4,6},{5,7},{6,4},{7,5},{8,10},{9,11},{10,... | collective-permute-start | bytes 589832 | tf_op jit(solution)/shard_map/ppermute | solution.py:17
  62.5 0.0 collective-permute-done.13
  62.5 5.4 %collective-permute-done.15 = bf16[48,2048]{1,0:T(8,128)(2,1)S(1)} collective-permute-done((bf16[48,2048]{1,0:T(8,128)(2,1)S(1)}, bf16[48,2048]{1,0:T(8,128)(2,1)S(1)}, u32[]{:S(2)}, u32[]{:S(2)}) %collective-permute-start.15) | collective-permute-done | bytes 196640 | tf_op jit(solution)/shard_map/ppermute | solution.py:17
  67.9 0.8 %add_convert_fusion = bf16[48,2048]{1,0:T(8,128)(2,1)} fusion(bf16[48,2048]{1,0:T(8,128)(2,1)S(1)} %collective-permute-done.15, bf16[48,2048]{1,0:T(8,128)(2,1)S(1)} %collective-permute-done.13, bf16[48,2048]{1,0:T(8,128)(2,1)S(1)} %get-tuple-element.37), kind=kLoop, calls=%fused_computation | loop fusion | flops 786432 | bytes 786432 | tf_op jit(solution)/shard_map/convert_element_type | solution.py:226
Async XLA Ops:
  0.0 8.1 %collective-permute-start = (bf16[48,2048]{1,0:T(8,128)(2,1)}, bf16[48,2048]{1,0:T(8,128)(2,1)S(1)}, u32[]{:S(2)}, u32[]{:S(2)}) collective-permute-start(bf16[48,2048]{1,0:T(8,128)(2,1)} %x_ref.1), channel_id=1, source_target_pairs={{0,2},{1,3},{2,0},{3,1},{4,6},{5,7},{6,4},{7,5},{8,10},{9,11},{10,... | collective-permute-start | bytes 589832 | tf_op jit(solution)/shard_map/ppermute | solution.py:17
  3.0 12.0 %collective-permute-start.1 = (bf16[48,2048]{1,0:T(8,128)(2,1)}, bf16[48,2048]{1,0:T(8,128)(2,1)S(1)}, u32[]{:S(2)}, u32[]{:S(2)}) collective-permute-start(bf16[48,2048]{1,0:T(8,128)(2,1)} %x_ref.1), channel_id=1, source_target_pairs={{0,1},{1,0},{2,3},{3,2},{4,5},{5,4},{6,7},{7,6},{8,9},{9,8},{10,11... | collective-permute-start | bytes 589832 | tf_op jit(solution)/shard_map/ppermute | solution.py:17
  8.1 6.9 %collective-permute-start.2 = (bf16[48,2048]{1,0:T(8,128)(2,1)S(1)}, bf16[48,2048]{1,0:T(8,128)(2,1)S(1)}, u32[]{:S(2)}, u32[]{:S(2)}) collective-permute-start(bf16[48,2048]{1,0:T(8,128)(2,1)S(1)} %collective-permute-done.refs_3_), channel_id=1, source_target_pairs={{0,1},{1,0},{2,3},{3,2},{4,5},{5,4},{6,7},{7,6},{8,9},{9,8},{10,11... | collective-permute-start | bytes 589832 | tf_op jit(solution)/shard_map/ppermute | solution.py:17
  8.1 1.6 %copy-start = (bf16[2048,512]{1,0:T(8,128)(2,1)S(1)}, bf16[2048,512]{1,0:T(8,128)(2,1)}, u32[]{:S(2)}) copy-start(bf16[2048,512]{1,0:T(8,128)(2,1)} %refs_6_.1) | copy-start | bytes 6291460
  9.7 1.6 %copy-start.2 = (bf16[2048,512]{1,0:T(8,128)(2,1)S(1)}, bf16[2048,512]{1,0:T(8,128)(2,1)}, u32[]{:S(2)}) copy-start(bf16[2048,512]{1,0:T(8,128)(2,1)} %refs_7_.1) | copy-start | bytes 6291460
  11.3 1.6 %copy-start.4 = (bf16[2048,512]{1,0:T(8,128)(2,1)S(1)}, bf16[2048,512]{1,0:T(8,128)(2,1)}, u32[]{:S(2)}) copy-start(bf16[2048,512]{1,0:T(8,128)(2,1)} %refs_8_.1) | copy-start | bytes 6291460
  12.9 0.9 %copy-start.9 = (bf16[48,2048]{1,0:T(8,128)(2,1)S(1)}, bf16[48,2048]{1,0:T(8,128)(2,1)}, u32[]{:S(2)}) copy-start(bf16[48,2048]{1,0:T(8,128)(2,1)} %x_ref.1) | copy-start | bytes 589828
  13.8 1.6 %copy-start.1 = (bf16[2048,512]{1,0:T(8,128)(2,1)S(1)}, bf16[2048,512]{1,0:T(8,128)(2,1)}, u32[]{:S(2)}) copy-start(bf16[2048,512]{1,0:T(8,128)(2,1)} %refs_6_.1) | copy-start | bytes 6291460
  13.8 2.2 %copy-start.3 = (bf16[2048,512]{1,0:T(8,128)(2,1)S(1)}, bf16[2048,512]{1,0:T(8,128)(2,1)}, u32[]{:S(2)}) copy-start(bf16[2048,512]{1,0:T(8,128)(2,1)} %refs_7_.1) | copy-start | bytes 6291460
  13.8 2.9 %copy-start.5 = (bf16[2048,512]{1,0:T(8,128)(2,1)S(1)}, bf16[2048,512]{1,0:T(8,128)(2,1)}, u32[]{:S(2)}) copy-start(bf16[2048,512]{1,0:T(8,128)(2,1)} %refs_8_.1) | copy-start | bytes 6291460
  16.7 24.1 %copy-start.7 = (f32[4]{0:T(128)S(1)}, f32[4]{0:T(128)}, u32[]{:S(2)}) copy-start(f32[4]{0:T(128)} %mix_ref.1) | copy-start | bytes 52
  16.7 24.1 %copy-start.8 = (f32[128]{0:T(128)S(1)}, f32[128]{0:T(128)}, u32[]{:S(2)}) copy-start(f32[128]{0:T(128)} %param.13) | copy-start | bytes 1540
  16.7 42.1 %copy-start.6 = (bf16[512,2048]{1,0:T(8,128)(2,1)S(1)}, bf16[512,2048]{1,0:T(8,128)(2,1)}, u32[]{:S(2)}) copy-start(bf16[512,2048]{1,0:T(8,128)(2,1)} %refs_4_.1) | copy-start | bytes 6291460
  18.3 12.9 %collective-permute-start.4 = (bf16[192,384]{1,0:T(8,128)(2,1)S(1)}, bf16[192,384]{1,0:T(8,128)(2,1)S(1)}, u32[]{:S(2)}, u32[]{:S(2)}) collective-permute-start(bf16[192,384]{1,0:T(8,128)(2,1)S(1)} %get-tuple-element.28), channel_id=1, source_target_pairs={{0,16},{4,20},{8,24},{12,28},{16,0},{20,4},{24,8},{28,12},{1,17},{... | collective-permute-start | bytes 442376 | tf_op jit(solution)/shard_map/ppermute | solution.py:17
  21.1 12.3 %collective-permute-start.6 = (bf16[192,256]{1,0:T(8,128)(2,1)S(1)}, bf16[192,256]{1,0:T(8,128)(2,1)S(1)}, u32[]{:S(2)}, u32[]{:S(2)}) collective-permute-start(bf16[192,256]{1,0:T(8,128)(2,1)S(1)} %get-tuple-element.30), channel_id=1, source_target_pairs={{0,28},{4,24},{8,20},{12,16},{16,12},{20,8},{24,4},{28,0},{1,29},{... | collective-permute-start | bytes 294920 | tf_op jit(solution)/shard_map/ppermute | solution.py:17
  23.4 17.3 %collective-permute-start.3 = (bf16[192,384]{1,0:T(8,128)(2,1)S(1)}, bf16[192,384]{1,0:T(8,128)(2,1)S(1)}, u32[]{:S(2)}, u32[]{:S(2)}) collective-permute-start(bf16[192,384]{1,0:T(8,128)(2,1)S(1)} %get-tuple-element.27), channel_id=1, source_target_pairs={{0,8},{4,12},{8,0},{12,4},{16,24},{20,28},{24,16},{28,20},{1,9},{5... | collective-permute-start | bytes 442376 | tf_op jit(solution)/shard_map/ppermute | solution.py:17
  23.4 17.3 %collective-permute-start.5 = (bf16[192,384]{1,0:T(8,128)(2,1)S(1)}, bf16[192,384]{1,0:T(8,128)(2,1)S(1)}, u32[]{:S(2)}, u32[]{:S(2)}) collective-permute-start(bf16[192,384]{1,0:T(8,128)(2,1)S(1)} %get-tuple-element.29), channel_id=1, source_target_pairs={{0,24},{4,28},{8,16},{12,20},{16,8},{20,12},{24,0},{28,4},{1,25},{... | collective-permute-start | bytes 442376 | tf_op jit(solution)/shard_map/ppermute | solution.py:17
  31.3 9.5 %collective-permute-start.9 = (bf16[192,384]{1,0:T(8,128)(2,1)S(1)}, bf16[192,384]{1,0:T(8,128)(2,1)S(1)}, u32[]{:S(2)}, u32[]{:S(2)}) collective-permute-start(bf16[192,384]{1,0:T(8,128)(2,1)S(1)} %collective-permute-done.4.refs_2_), channel_id=1, source_target_pairs={{0,4},{4,0},{8,12},{12,8},{16,20},{20,16},{24,28},{28,24},{1,5},{5... | collective-permute-start | bytes 442376 | tf_op jit(solution)/shard_map/ppermute | solution.py:17
  33.0 5.6 %collective-permute-start.7 = (bf16[192,256]{1,0:T(8,128)(2,1)S(1)}, bf16[192,256]{1,0:T(8,128)(2,1)S(1)}, u32[]{:S(2)}, u32[]{:S(2)}) collective-permute-start(bf16[192,256]{1,0:T(8,128)(2,1)S(1)} %get-tuple-element.31), channel_id=1, source_target_pairs={{0,12},{4,8},{8,4},{12,0},{16,28},{20,24},{24,20},{28,16},{1,13},{... | collective-permute-start | bytes 294920 | tf_op jit(solution)/shard_map/ppermute | solution.py:17
  33.5 7.3 %collective-permute-start.8 = (bf16[192,256]{1,0:T(8,128)(2,1)S(1)}, bf16[192,256]{1,0:T(8,128)(2,1)S(1)}, u32[]{:S(2)}, u32[]{:S(2)}) collective-permute-start(bf16[192,256]{1,0:T(8,128)(2,1)S(1)} %get-tuple-element.32), channel_id=1, source_target_pairs={{0,4},{4,0},{8,12},{12,8},{16,20},{20,16},{24,28},{28,24},{1,5},{5... | collective-permute-start | bytes 294920 | tf_op jit(solution)/shard_map/ppermute | solution.py:17
  47.1 7.0 %collective-permute-start.10 = (bf16[192,128]{1,0:T(8,128)(2,1)S(1)}, bf16[192,128]{1,0:T(8,128)(2,1)S(1)}, u32[]{:S(2)}, u32[]{:S(2)}) collective-permute-start(bf16[192,128]{1,0:T(8,128)(2,1)S(1)} %get-tuple-element.34), channel_id=1, source_target_pairs={{0,8},{4,12},{8,0},{12,4},{16,24},{20,28},{24,16},{28,20},{1,9},{5... | collective-permute-start | bytes 147464 | tf_op jit(solution)/shard_map/ppermute | solution.py:17
  50.0 5.2 %collective-permute-start.11 = (bf16[192,128]{1,0:T(8,128)(2,1)S(1)}, bf16[192,128]{1,0:T(8,128)(2,1)S(1)}, u32[]{:S(2)}, u32[]{:S(2)}) collective-permute-start(bf16[192,128]{1,0:T(8,128)(2,1)S(1)} %get-tuple-element.35), channel_id=1, source_target_pairs={{0,16},{4,20},{8,24},{12,28},{16,0},{20,4},{24,8},{28,12},{1,17},{... | collective-permute-start | bytes 147464 | tf_op jit(solution)/shard_map/ppermute | solution.py:17
  52.7 6.0 %collective-permute-start.12 = (bf16[192,128]{1,0:T(8,128)(2,1)S(1)}, bf16[192,128]{1,0:T(8,128)(2,1)S(1)}, u32[]{:S(2)}, u32[]{:S(2)}) collective-permute-start(bf16[192,128]{1,0:T(8,128)(2,1)S(1)} %get-tuple-element.36), channel_id=1, source_target_pairs={{0,24},{4,28},{8,16},{12,20},{16,8},{20,12},{24,0},{28,4},{1,25},{... | collective-permute-start | bytes 147464 | tf_op jit(solution)/shard_map/ppermute | solution.py:17
  59.4 1.5 %collective-permute-start.14 = (bf16[48,2048]{1,0:T(8,128)(2,1)S(1)}, bf16[48,2048]{1,0:T(8,128)(2,1)S(1)}, u32[]{:S(2)}, u32[]{:S(2)}) collective-permute-start(bf16[48,2048]{1,0:T(8,128)(2,1)S(1)} %get-tuple-element.40), channel_id=1, source_target_pairs={{0,1},{1,0},{2,3},{3,2},{4,5},{5,4},{6,7},{7,6},{8,9},{9,8},{10,11... | collective-permute-start | bytes 589832 | tf_op jit(solution)/shard_map/ppermute | solution.py:17
  59.4 3.1 %collective-permute-start.13 = (bf16[48,2048]{1,0:T(8,128)(2,1)S(1)}, bf16[48,2048]{1,0:T(8,128)(2,1)S(1)}, u32[]{:S(2)}, u32[]{:S(2)}) collective-permute-start(bf16[48,2048]{1,0:T(8,128)(2,1)S(1)} %get-tuple-element.38), channel_id=1, source_target_pairs={{0,1},{1,0},{2,3},{3,2},{4,5},{5,4},{6,7},{7,6},{8,9},{9,8},{10,11... | collective-permute-start | bytes 589832 | tf_op jit(solution)/shard_map/ppermute | solution.py:17
  60.9 7.0 %collective-permute-start.15 = (bf16[48,2048]{1,0:T(8,128)(2,1)S(1)}, bf16[48,2048]{1,0:T(8,128)(2,1)S(1)}, u32[]{:S(2)}, u32[]{:S(2)}) collective-permute-start(bf16[48,2048]{1,0:T(8,128)(2,1)S(1)} %add_convert_fusion.1), channel_id=1, source_target_pairs={{0,2},{1,3},{2,0},{3,1},{4,6},{5,7},{6,4},{7,5},{8,10},{9,11},{10,... | collective-permute-start | bytes 589832 | tf_op jit(solution)/shard_map/ppermute | solution.py:17
where the time goes:
time: 68.9 us; the launch traced here: 68.7 us
  waiting for transfers between devices  26.5 us (38%)
  starting transfers between devices  24.1 us (35%)
  Pallas kernels  9.75 us (14%)
  local copies, waits for them, and re-layouts  7.37 us (11%)
  other arithmetic  0.8 us (1%)
    ppermute x16, waiting for transfers between devices, swap(): return lax.ppermute(array, axis, [(i, i ^ mask) for i in range(size)])  26.5 us
    ppermute x16, starting transfers between devices, swap(): return lax.ppermute(array, axis, [(i, i ^ mask) for i in range(size)])  24.1 us
    unnamed x20, local copies, waits for them, and re-layouts  7.37 us
    pallas_call x1, Pallas kernels, attend(): pl.pallas_call(body, out_shape=[jax.ShapeDtypeStruct((rows, vd), BF16)] *...  6.32 us
    pallas_call x1, Pallas kernels, project(): pl.pallas_call(body, out_shape=shapes, in_specs=[VMEM] * (n + 6), out_spe...  1.66 us
  transfers between devices with their start and end apart: 16, of which 8 were waited for; matrix products, arithmetic and copies ran while one was open for 0% of the time, Pallas kernels for 2%

commit v1 on v0

--- a/solution.py
+++ b/solution.py
@@ -84,7 +84,7 @@
     n = len(parts)
     queries, keys = nq * rows, n * rows
     half = qk // 2
-    block = 256 if queries % 256 == 0 else rows
+    block = next((b for b in (256, 384, 128) if queries % b == 0), rows)
     chunk = max(c * rows for c in range(1, n + 1) if n % c == 0 and c * rows <= 2048)
     factor = half**-0.5 * LOG2E
 
@@ -217,8 +217,17 @@
             for r in range(1, sharing):
                 kv_parts[relay, r] = swap(q_parts[relay], "sp", n_sp, r)
         kv_parts = list(kv_parts.values())
-        out = attend(q_parts, kv_parts, mix_weight, out_gain, sharing, qk, vd)
-        normed = [out[0]] + [swap(out[j], "sp", n_sp, j * sharing) for j in range(1, heads)]
+        cut = (heads + 1) // 2
+        normed = [None] * heads
+        for js in (range(cut, heads), range(cut)):
+            if not js:
+                continue
+            rest = [p for j, p in enumerate(q_parts) if j not in js]
+            out = attend(
+                [q_parts[j] for j in js], rest + kv_parts, mix_weight, out_gain, sharing, qk, vd
+            )
+            for j, o in zip(js, out):
+                normed[j] = swap(o, "sp", n_sp, j * sharing) if j else o
         parts = dict(zip(masks, project_out(normed, w_out, sharing, masks, rows)))
         for bit in bits:
             moved = {m: swap(p, "tp", n_tp, bit) for m, p in parts.items() if m & bit}

time: 68.9 us -> 66.1 us (0.959)
  waiting for transfers between devices: 26.5 us -> 25.4 us
  Pallas kernels: 9.75 us -> 8.9 us
  starting transfers between devices: 24.1 us -> 23.4 us
    ppermute x16, waiting for transfers between devices: 26.5 us -> 25.4 us  [swap(): return lax.ppermute(array, axis, [(i, i ^ mask) for i in range(size)])]
    pallas_call x1 -> x2, Pallas kernels: 6.32 us -> 5.47 us  [attend(): pl.pallas_call(body, out_shape=[jax.ShapeDtypeStruct((rows, vd), BF16)] *...]
    ppermute x16, starting transfers between devices: 24.1 us -> 23.4 us  [swap(): return lax.ppermute(array, axis, [(i, i ^ mask) for i in range(size)])]
  transfers between devices with their start and end apart: 16 -> 16, of which waited for: 8 -> 8; matrix products, arithmetic and copies ran while one was open for 0% -> 0% of each run, Pallas kernels for 2% -> 6%
where the time goes in v1:
time: 66.1 us; the launch traced here: 65.9 us
  waiting for transfers between devices  25.4 us (38%)
  starting transfers between devices  23.4 us (35%)
  Pallas kernels  8.9 us (13%)
  local copies, waits for them, and re-layouts  7.37 us (11%)
  other arithmetic  0.8 us (1%)
    ppermute x16, waiting for transfers between devices, swap(): return lax.ppermute(array, axis, [(i, i ^ mask) for i in range(size)])  25.4 us
    ppermute x16, starting transfers between devices, swap(): return lax.ppermute(array, axis, [(i, i ^ mask) for i in range(size)])  23.4 us
    unnamed x20, local copies, waits for them, and re-layouts  7.37 us
    pallas_call x2, Pallas kernels, attend(): pl.pallas_call(body, out_shape=[jax.ShapeDtypeStruct((rows, vd), BF16)] *...  5.47 us
    pallas_call x1, Pallas kernels, project(): pl.pallas_call(body, out_shape=shapes, in_specs=[VMEM] * (n + 6), out_spe...  1.66 us
  transfers between devices with their start and end apart: 16, of which 8 were waited for; matrix products, arithmetic and copies ran while one was open for 0% of the time, Pallas kernels for 6%

profile of v1, /device:TPU:0, one launch (start us, length us, event | category | flops | bytes accessed | tf_op | source)
XLA Modules:
  0.0 65.9 jit_solution(14893043705596388440)
XLA Ops:
  0.0 3.0 %collective-permute-start = (bf16[48,2048]{1,0:T(8,128)(2,1)}, bf16[48,2048]{1,0:T(8,128)(2,1)S(1)}, u32[]{:S(2)}, u32[]{:S(2)}) collective-permute-start(bf16[48,2048]{1,0:T(8,128)(2,1)} %x_ref.1), channel_id=1, source_target_pairs={{0,2},{1,3},{2,0},{3,1},{4,6},{5,7},{6,4},{7,5},{8,10},{9,11},{10,... | collective-permute-start | bytes 589832 | tf_op jit(solution)/shard_map/ppermute | solution.py:17
  3.0 0.0 collective-permute-start.1
  3.0 5.1 %collective-permute-done.refs_3_ = bf16[48,2048]{1,0:T(8,128)(2,1)S(1)} collective-permute-done((bf16[48,2048]{1,0:T(8,128)(2,1)}, bf16[48,2048]{1,0:T(8,128)(2,1)S(1)}, u32[]{:S(2)}, u32[]{:S(2)}) %collective-permute-start) | collective-permute-done | bytes 196640 | tf_op jit(solution)/shard_map/ppermute | solution.py:17
  8.1 0.0 collective-permute-start.2
  8.1 0.0 copy-start
  8.1 1.6 %copy-done = bf16[2048,512]{1,0:T(8,128)(2,1)S(1)} copy-done((bf16[2048,512]{1,0:T(8,128)(2,1)S(1)}, bf16[2048,512]{1,0:T(8,128)(2,1)}, u32[]{:S(2)}) %copy-start) | copy-done | bytes 2097176
  9.7 0.0 copy-start.2
  9.7 1.6 %copy-done.2 = bf16[2048,512]{1,0:T(8,128)(2,1)S(1)} copy-done((bf16[2048,512]{1,0:T(8,128)(2,1)S(1)}, bf16[2048,512]{1,0:T(8,128)(2,1)}, u32[]{:S(2)}) %copy-start.2) | copy-done | bytes 2097176
  11.3 0.0 copy-start.4
  11.3 1.6 %copy-done.4 = bf16[2048,512]{1,0:T(8,128)(2,1)S(1)} copy-done((bf16[2048,512]{1,0:T(8,128)(2,1)S(1)}, bf16[2048,512]{1,0:T(8,128)(2,1)}, u32[]{:S(2)}) %copy-start.4) | copy-done | bytes 2097176
  12.9 0.0 copy-start.9
  12.9 0.9 %copy-done.9 = bf16[48,2048]{1,0:T(8,128)(2,1)S(1)} copy-done((bf16[48,2048]{1,0:T(8,128)(2,1)S(1)}, bf16[48,2048]{1,0:T(8,128)(2,1)}, u32[]{:S(2)}) %copy-start.9) | copy-done | bytes 196632
  13.8 0.0 copy-start.1
  13.8 0.0 copy-start.3
  13.8 0.0 copy-start.5
  13.8 1.2 %project_own.1 = (bf16[48,512]{1,0:T(8,128)(2,1)S(1)}, bf16[48,512]{1,0:T(8,128)(2,1)S(1)}, bf16[48,512]{1,0:T(8,128)(2,1)S(1)}) custom-call(bf16[48,2048]{1,0:T(8,128)(2,1)S(1)} %copy-done.9, bf16[2048,512]{1,0:T(8,128)(2,1)S(1)} %copy-done, bf16[2048,512]{1,0:T(8,128)(2,1)S(1)} %copy-done.2, bf16[2048,512]{1,0:T(8,128)(2,1)S(1)} %copy-done.4), custom_call_target="tpu_custom_call" | custom-call | flops 2415919104 | bytes 6291456 | tf_op jit(solution)/shard_map/project_own/pallas_call | solution.py:28
  15.0 0.0 collective-permute-done.1.refs_4_
  15.0 0.0 collective-permute-done.2.refs_5_
  15.0 0.4 copy-done.1
  15.4 0.6 copy-done.3
  16.0 0.6 copy-done.5
  16.7 0.0 copy-start.7
  16.7 0.0 copy-start.8
  16.7 0.0 copy-start.6
  16.7 1.7 %project.1 = (bf16[192,384]{1,0:T(8,128)(2,1)S(1)}, bf16[192,384]{1,0:T(8,128)(2,1)S(1)}, bf16[192,384]{1,0:T(8,128)(2,1)S(1)}, bf16[192,384]{1,0:T(8,128)(2,1)S...) custom-call(bf16[48,512]{1,0:T(8,128)(2,1)S(1)} %get-tuple-element.2, ...), custom_call_target="tpu_custom_call" | custom-call | tf_op jit(solution)/shard_map/project/pallas_call | solution.py:69
  18.3 2.8 %collective-permute-start.4 = (bf16[192,384]{1,0:T(8,128)(2,1)S(1)}, bf16[192,384]{1,0:T(8,128)(2,1)S(1)}, u32[]{:S(2)}, u32[]{:S(2)}) collective-permute-start(bf16[192,384]{1,0:T(8,128)(2,1)S(1)} %get-tuple-element.28), channel_id=1, source_target_pairs={{0,16},{4,20},{8,24},{12,28},{16,0},{20,4},{24,8},{28,12},{1,17},{... | collective-permute-start | bytes 442376 | tf_op jit(solution)/shard_map/ppermute | solution.py:17
  21.1 2.3 %collective-permute-start.6 = (bf16[192,256]{1,0:T(8,128)(2,1)S(1)}, bf16[192,256]{1,0:T(8,128)(2,1)S(1)}, u32[]{:S(2)}, u32[]{:S(2)}) collective-permute-start(bf16[192,256]{1,0:T(8,128)(2,1)S(1)} %get-tuple-element.30), channel_id=1, source_target_pairs={{0,28},{4,24},{8,20},{12,16},{16,12},{20,8},{24,4},{28,0},{1,29},{... | collective-permute-start | bytes 294920 | tf_op jit(solution)/shard_map/ppermute | solution.py:17
  23.4 0.0 collective-permute-start.3
  23.4 3.2 %collective-permute-start.5 = (bf16[192,384]{1,0:T(8,128)(2,1)S(1)}, bf16[192,384]{1,0:T(8,128)(2,1)S(1)}, u32[]{:S(2)}, u32[]{:S(2)}) collective-permute-start(bf16[192,384]{1,0:T(8,128)(2,1)S(1)} %get-tuple-element.29), channel_id=1, source_target_pairs={{0,24},{4,28},{8,16},{12,20},{16,8},{20,12},{24,0},{28,4},{1,25},{... | collective-permute-start | bytes 442376 | tf_op jit(solution)/shard_map/ppermute | solution.py:17
  26.6 4.7 %collective-permute-done.4.refs_2_.refs_0_ = bf16[192,384]{1,0:T(8,128)(2,1)S(1)} collective-permute-done((bf16[192,384]{1,0:T(8,128)(2,1)S(1)}, bf16[192,384]{1,0:T(8,128)(2,1)S(1)}, u32[]{:S(2)}, u32[]{:S(2)}) %collective-permute-start.4) | collective-permute-done | bytes 147488 | tf_op jit(solution)/shard_map/ppermute | solution.py:17
  31.3 1.7 %collective-permute-start.9 = (bf16[192,384]{1,0:T(8,128)(2,1)S(1)}, bf16[192,384]{1,0:T(8,128)(2,1)S(1)}, u32[]{:S(2)}, u32[]{:S(2)}) collective-permute-start(bf16[192,384]{1,0:T(8,128)(2,1)S(1)} %collective-permute-done.4.refs_2_.refs_0_), channel_id=1, source_target_pairs={{0,4},{4,0},{8,12},{12,8},{16,20},{20,16},{24,28},{28,24},{1,5},{5... | collective-permute-start | bytes 442376 | tf_op jit(solution)/shard_map/ppermute | solution.py:17
  33.0 0.5 collective-permute-start.7
  33.5 0.0 collective-permute-done.6.refs_4_
  33.5 1.5 %collective-permute-start.8 = (bf16[192,256]{1,0:T(8,128)(2,1)S(1)}, bf16[192,256]{1,0:T(8,128)(2,1)S(1)}, u32[]{:S(2)}, u32[]{:S(2)}) collective-permute-start(bf16[192,256]{1,0:T(8,128)(2,1)S(1)} %get-tuple-element.32), channel_id=1, source_target_pairs={{0,4},{4,0},{8,12},{12,8},{16,20},{20,16},{24,28},{28,24},{1,5},{5... | collective-permute-start | bytes 294920 | tf_op jit(solution)/shard_map/ppermute | solution.py:17
  35.0 3.6 %collective-permute-done.7.refs_5_ = bf16[192,256]{1,0:T(8,128)(2,1)S(1)} collective-permute-done((bf16[192,256]{1,0:T(8,128)(2,1)S(1)}, bf16[192,256]{1,0:T(8,128)(2,1)S(1)}, u32[]{:S(2)}, u32[]{:S(2)}) %collective-permute-start.7) | collective-permute-done | bytes 98336 | tf_op jit(solution)/shard_map/ppermute | solution.py:17
  38.6 2.1 %collective-permute-done.8.refs_6_ = bf16[192,256]{1,0:T(8,128)(2,1)S(1)} collective-permute-done((bf16[192,256]{1,0:T(8,128)(2,1)S(1)}, bf16[192,256]{1,0:T(8,128)(2,1)S(1)}, u32[]{:S(2)}, u32[]{:S(2)}) %collective-permute-start.8) | collective-permute-done | bytes 98336 | tf_op jit(solution)/shard_map/ppermute | solution.py:17
  40.8 0.0 collective-permute-done.3.refs_1_.refs_3_
  40.8 0.0 collective-permute-done.5.refs_3_.refs_1_
  40.8 0.0 collective-permute-done.9.refs_7_
  40.8 0.0 copy-done.7
  40.8 0.0 copy-done.8
  40.8 2.7 %attend.3 = (bf16[192,128]{1,0:T(8,128)(2,1)S(1)}, bf16[192,128]{1,0:T(8,128)(2,1)S(1)}) custom-call(f32[4]{0:T(128)S(1)} %copy-done.7, f32[1,128]{1,0:T(1,128)S(1)} %bitcast.1, bf16[192,384]{1,0:T(8,128)(2,1)S(1)} %collective-permute-done.4.refs_2_.refs_0_, bf16[192,384]{1,0:T(8,128)(2,1)S(1)} %collective-permute-done.5.refs_3_.refs_1_, ...), custom_call_target="tpu_custom_call" | custom-call | tf_op jit(solution)/shard_map/attend/pallas_call | solution.py:146
  43.5 5.5 %collective-permute-start.11 = (bf16[192,128]{1,0:T(8,128)(2,1)S(1)}, bf16[192,128]{1,0:T(8,128)(2,1)S(1)}, u32[]{:S(2)}, u32[]{:S(2)}) collective-permute-start(bf16[192,128]{1,0:T(8,128)(2,1)S(1)} %get-tuple-element.35), channel_id=1, source_target_pairs={{0,16},{4,20},{8,24},{12,28},{16,0},{20,4},{24,8},{28,12},{1,17},{... | collective-permute-start | bytes 147464 | tf_op jit(solution)/shard_map/ppermute | solution.py:17
  49.1 0.0 collective-permute-start.12
  49.1 2.7 %attend.2 = (bf16[192,128]{1,0:T(8,128)(2,1)S(1)}, bf16[192,128]{1,0:T(8,128)(2,1)S(1)}) custom-call(f32[4]{0:T(128)S(1)} %copy-done.7, f32[1,128]{1,0:T(1,128)S(1)} %bitcast.2, bf16[192,384]{1,0:T(8,128)(2,1)S(1)} %get-tuple-element.26.refs_0_.refs_2_, bf16[192,384]{1,0:T(8,128)(2,1)S(1)} %collective-permute-done.3.refs_1_.refs_3_, ...), custom_call_target="tpu_custom_call" | custom-call | tf_op jit(solution)/shard_map/attend/pallas_call | solution.py:146
  51.8 0.7 %collective-permute-start.10 = (bf16[192,128]{1,0:T(8,128)(2,1)S(1)}, bf16[192,128]{1,0:T(8,128)(2,1)S(1)}, u32[]{:S(2)}, u32[]{:S(2)}) collective-permute-start(bf16[192,128]{1,0:T(8,128)(2,1)S(1)} %get-tuple-element.34), channel_id=1, source_target_pairs={{0,8},{4,12},{8,0},{12,4},{16,24},{20,28},{24,16},{28,20},{1,9},{5... | collective-permute-start | bytes 147464 | tf_op jit(solution)/shard_map/ppermute | solution.py:17
  52.5 0.0 collective-permute-done.11.refs_2_
  52.5 2.8 %collective-permute-done.12.refs_3_ = bf16[192,128]{1,0:T(8,128)(2,1)S(1)} collective-permute-done((bf16[192,128]{1,0:T(8,128)(2,1)S(1)}, bf16[192,128]{1,0:T(8,128)(2,1)S(1)}, u32[]{:S(2)}, u32[]{:S(2)}) %collective-permute-start.12) | collective-permute-done | bytes 49184 | tf_op jit(solution)/shard_map/ppermute | solution.py:17
  55.3 0.6 collective-permute-done.10.refs_1_
  56.0 0.0 copy-done.6
  56.0 0.6 project_out.1
  56.6 0.1 collective-permute-start.14
  56.7 0.5 collective-permute-start.13
  57.2 0.9 %collective-permute-done.14 = bf16[48,2048]{1,0:T(8,128)(2,1)S(1)} collective-permute-done((bf16[48,2048]{1,0:T(8,128)(2,1)S(1)}, bf16[48,2048]{1,0:T(8,128)(2,1)S(1)}, u32[]{:S(2)}, u32[]{:S(2)}) %collective-permute-start.14) | collective-permute-done | bytes 196640 | tf_op jit(solution)/shard_map/ppermute | solution.py:17
  58.1 0.1 add_convert_fusion.1
  58.1 1.6 %collective-permute-start.15 = (bf16[48,2048]{1,0:T(8,128)(2,1)S(1)}, bf16[48,2048]{1,0:T(8,128)(2,1)S(1)}, u32[]{:S(2)}, u32[]{:S(2)}) collective-permute-start(bf16[48,2048]{1,0:T(8,128)(2,1)S(1)} %add_convert_fusion.1), channel_id=1, source_target_pairs={{0,2},{1,3},{2,0},{3,1},{4,6},{5,7},{6,4},{7,5},{8,10},{9,11},{10,... | collective-permute-start | bytes 589832 | tf_op jit(solution)/shard_map/ppermute | solution.py:17
  59.7 0.0 collective-permute-done.13
  59.7 5.4 %collective-permute-done.15 = bf16[48,2048]{1,0:T(8,128)(2,1)S(1)} collective-permute-done((bf16[48,2048]{1,0:T(8,128)(2,1)S(1)}, bf16[48,2048]{1,0:T(8,128)(2,1)S(1)}, u32[]{:S(2)}, u32[]{:S(2)}) %collective-permute-start.15) | collective-permute-done | bytes 196640 | tf_op jit(solution)/shard_map/ppermute | solution.py:17
  65.2 0.8 %add_convert_fusion = bf16[48,2048]{1,0:T(8,128)(2,1)} fusion(bf16[48,2048]{1,0:T(8,128)(2,1)S(1)} %collective-permute-done.15, bf16[48,2048]{1,0:T(8,128)(2,1)S(1)} %collective-permute-done.13, bf16[48,2048]{1,0:T(8,128)(2,1)S(1)} %get-tuple-element.37), kind=kLoop, calls=%fused_computation | loop fusion | flops 786432 | bytes 786432 | tf_op jit(solution)/shard_map/convert_element_type | solution.py:235
Async XLA Ops:
  0.0 8.1 %collective-permute-start = (bf16[48,2048]{1,0:T(8,128)(2,1)}, bf16[48,2048]{1,0:T(8,128)(2,1)S(1)}, u32[]{:S(2)}, u32[]{:S(2)}) collective-permute-start(bf16[48,2048]{1,0:T(8,128)(2,1)} %x_ref.1), channel_id=1, source_target_pairs={{0,2},{1,3},{2,0},{3,1},{4,6},{5,7},{6,4},{7,5},{8,10},{9,11},{10,... | collective-permute-start | bytes 589832 | tf_op jit(solution)/shard_map/ppermute | solution.py:17
  3.0 12.0 %collective-permute-start.1 = (bf16[48,2048]{1,0:T(8,128)(2,1)}, bf16[48,2048]{1,0:T(8,128)(2,1)S(1)}, u32[]{:S(2)}, u32[]{:S(2)}) collective-permute-start(bf16[48,2048]{1,0:T(8,128)(2,1)} %x_ref.1), channel_id=1, source_target_pairs={{0,1},{1,0},{2,3},{3,2},{4,5},{5,4},{6,7},{7,6},{8,9},{9,8},{10,11... | collective-permute-start | bytes 589832 | tf_op jit(solution)/shard_map/ppermute | solution.py:17
  8.1 6.9 %collective-permute-start.2 = (bf16[48,2048]{1,0:T(8,128)(2,1)S(1)}, bf16[48,2048]{1,0:T(8,128)(2,1)S(1)}, u32[]{:S(2)}, u32[]{:S(2)}) collective-permute-start(bf16[48,2048]{1,0:T(8,128)(2,1)S(1)} %collective-permute-done.refs_3_), channel_id=1, source_target_pairs={{0,1},{1,0},{2,3},{3,2},{4,5},{5,4},{6,7},{7,6},{8,9},{9,8},{10,11... | collective-permute-start | bytes 589832 | tf_op jit(solution)/shard_map/ppermute | solution.py:17
  8.1 1.6 %copy-start = (bf16[2048,512]{1,0:T(8,128)(2,1)S(1)}, bf16[2048,512]{1,0:T(8,128)(2,1)}, u32[]{:S(2)}) copy-start(bf16[2048,512]{1,0:T(8,128)(2,1)} %refs_6_.1) | copy-start | bytes 6291460
  9.7 1.6 %copy-start.2 = (bf16[2048,512]{1,0:T(8,128)(2,1)S(1)}, bf16[2048,512]{1,0:T(8,128)(2,1)}, u32[]{:S(2)}) copy-start(bf16[2048,512]{1,0:T(8,128)(2,1)} %refs_7_.1) | copy-start | bytes 6291460
  11.3 1.6 %copy-start.4 = (bf16[2048,512]{1,0:T(8,128)(2,1)S(1)}, bf16[2048,512]{1,0:T(8,128)(2,1)}, u32[]{:S(2)}) copy-start(bf16[2048,512]{1,0:T(8,128)(2,1)} %refs_8_.1) | copy-start | bytes 6291460
  12.9 0.9 %copy-start.9 = (bf16[48,2048]{1,0:T(8,128)(2,1)S(1)}, bf16[48,2048]{1,0:T(8,128)(2,1)}, u32[]{:S(2)}) copy-start(bf16[48,2048]{1,0:T(8,128)(2,1)} %x_ref.1) | copy-start | bytes 589828
  13.8 1.6 %copy-start.1 = (bf16[2048,512]{1,0:T(8,128)(2,1)S(1)}, bf16[2048,512]{1,0:T(8,128)(2,1)}, u32[]{:S(2)}) copy-start(bf16[2048,512]{1,0:T(8,128)(2,1)} %refs_6_.1) | copy-start | bytes 6291460
  13.8 2.2 %copy-start.3 = (bf16[2048,512]{1,0:T(8,128)(2,1)S(1)}, bf16[2048,512]{1,0:T(8,128)(2,1)}, u32[]{:S(2)}) copy-start(bf16[2048,512]{1,0:T(8,128)(2,1)} %refs_7_.1) | copy-start | bytes 6291460
  13.8 2.9 %copy-start.5 = (bf16[2048,512]{1,0:T(8,128)(2,1)S(1)}, bf16[2048,512]{1,0:T(8,128)(2,1)}, u32[]{:S(2)}) copy-start(bf16[2048,512]{1,0:T(8,128)(2,1)} %refs_8_.1) | copy-start | bytes 6291460
  16.7 24.1 %copy-start.7 = (f32[4]{0:T(128)S(1)}, f32[4]{0:T(128)}, u32[]{:S(2)}) copy-start(f32[4]{0:T(128)} %mix_ref.3) | copy-start | bytes 52
  16.7 24.1 %copy-start.8 = (f32[128]{0:T(128)S(1)}, f32[128]{0:T(128)}, u32[]{:S(2)}) copy-start(f32[128]{0:T(128)} %param.13) | copy-start | bytes 1540
  16.7 39.3 %copy-start.6 = (bf16[512,2048]{1,0:T(8,128)(2,1)S(1)}, bf16[512,2048]{1,0:T(8,128)(2,1)}, u32[]{:S(2)}) copy-start(bf16[512,2048]{1,0:T(8,128)(2,1)} %refs_4_.1) | copy-start | bytes 6291460
  18.3 12.9 %collective-permute-start.4 = (bf16[192,384]{1,0:T(8,128)(2,1)S(1)}, bf16[192,384]{1,0:T(8,128)(2,1)S(1)}, u32[]{:S(2)}, u32[]{:S(2)}) collective-permute-start(bf16[192,384]{1,0:T(8,128)(2,1)S(1)} %get-tuple-element.28), channel_id=1, source_target_pairs={{0,16},{4,20},{8,24},{12,28},{16,0},{20,4},{24,8},{28,12},{1,17},{... | collective-permute-start | bytes 442376 | tf_op jit(solution)/shard_map/ppermute | solution.py:17
  21.1 12.3 %collective-permute-start.6 = (bf16[192,256]{1,0:T(8,128)(2,1)S(1)}, bf16[192,256]{1,0:T(8,128)(2,1)S(1)}, u32[]{:S(2)}, u32[]{:S(2)}) collective-permute-start(bf16[192,256]{1,0:T(8,128)(2,1)S(1)} %get-tuple-element.30), channel_id=1, source_target_pairs={{0,28},{4,24},{8,20},{12,16},{16,12},{20,8},{24,4},{28,0},{1,29},{... | collective-permute-start | bytes 294920 | tf_op jit(solution)/shard_map/ppermute | solution.py:17
  23.4 17.3 %collective-permute-start.3 = (bf16[192,384]{1,0:T(8,128)(2,1)S(1)}, bf16[192,384]{1,0:T(8,128)(2,1)S(1)}, u32[]{:S(2)}, u32[]{:S(2)}) collective-permute-start(bf16[192,384]{1,0:T(8,128)(2,1)S(1)} %get-tuple-element.27), channel_id=1, source_target_pairs={{0,8},{4,12},{8,0},{12,4},{16,24},{20,28},{24,16},{28,20},{1,9},{5... | collective-permute-start | bytes 442376 | tf_op jit(solution)/shard_map/ppermute | solution.py:17
  23.4 17.3 %collective-permute-start.5 = (bf16[192,384]{1,0:T(8,128)(2,1)S(1)}, bf16[192,384]{1,0:T(8,128)(2,1)S(1)}, u32[]{:S(2)}, u32[]{:S(2)}) collective-permute-start(bf16[192,384]{1,0:T(8,128)(2,1)S(1)} %get-tuple-element.29), channel_id=1, source_target_pairs={{0,24},{4,28},{8,16},{12,20},{16,8},{20,12},{24,0},{28,4},{1,25},{... | collective-permute-start | bytes 442376 | tf_op jit(solution)/shard_map/ppermute | solution.py:17
  31.3 9.5 %collective-permute-start.9 = (bf16[192,384]{1,0:T(8,128)(2,1)S(1)}, bf16[192,384]{1,0:T(8,128)(2,1)S(1)}, u32[]{:S(2)}, u32[]{:S(2)}) collective-permute-start(bf16[192,384]{1,0:T(8,128)(2,1)S(1)} %collective-permute-done.4.refs_2_.refs_0_), channel_id=1, source_target_pairs={{0,4},{4,0},{8,12},{12,8},{16,20},{20,16},{24,28},{28,24},{1,5},{5... | collective-permute-start | bytes 442376 | tf_op jit(solution)/shard_map/ppermute | solution.py:17
  33.0 5.6 %collective-permute-start.7 = (bf16[192,256]{1,0:T(8,128)(2,1)S(1)}, bf16[192,256]{1,0:T(8,128)(2,1)S(1)}, u32[]{:S(2)}, u32[]{:S(2)}) collective-permute-start(bf16[192,256]{1,0:T(8,128)(2,1)S(1)} %get-tuple-element.31), channel_id=1, source_target_pairs={{0,12},{4,8},{8,4},{12,0},{16,28},{20,24},{24,20},{28,16},{1,13},{... | collective-permute-start | bytes 294920 | tf_op jit(solution)/shard_map/ppermute | solution.py:17
  33.5 7.3 %collective-permute-start.8 = (bf16[192,256]{1,0:T(8,128)(2,1)S(1)}, bf16[192,256]{1,0:T(8,128)(2,1)S(1)}, u32[]{:S(2)}, u32[]{:S(2)}) collective-permute-start(bf16[192,256]{1,0:T(8,128)(2,1)S(1)} %get-tuple-element.32), channel_id=1, source_target_pairs={{0,4},{4,0},{8,12},{12,8},{16,20},{20,16},{24,28},{28,24},{1,5},{5... | collective-permute-start | bytes 294920 | tf_op jit(solution)/shard_map/ppermute | solution.py:17
  43.5 9.0 %collective-permute-start.11 = (bf16[192,128]{1,0:T(8,128)(2,1)S(1)}, bf16[192,128]{1,0:T(8,128)(2,1)S(1)}, u32[]{:S(2)}, u32[]{:S(2)}) collective-permute-start(bf16[192,128]{1,0:T(8,128)(2,1)S(1)} %get-tuple-element.35), channel_id=1, source_target_pairs={{0,16},{4,20},{8,24},{12,28},{16,0},{20,4},{24,8},{28,12},{1,17},{... | collective-permute-start | bytes 147464 | tf_op jit(solution)/shard_map/ppermute | solution.py:17
  49.1 6.2 %collective-permute-start.12 = (bf16[192,128]{1,0:T(8,128)(2,1)S(1)}, bf16[192,128]{1,0:T(8,128)(2,1)S(1)}, u32[]{:S(2)}, u32[]{:S(2)}) collective-permute-start(bf16[192,128]{1,0:T(8,128)(2,1)S(1)} %get-tuple-element.36), channel_id=1, source_target_pairs={{0,24},{4,28},{8,16},{12,20},{16,8},{20,12},{24,0},{28,4},{1,25},{... | collective-permute-start | bytes 147464 | tf_op jit(solution)/shard_map/ppermute | solution.py:17
  51.8 4.2 %collective-permute-start.10 = (bf16[192,128]{1,0:T(8,128)(2,1)S(1)}, bf16[192,128]{1,0:T(8,128)(2,1)S(1)}, u32[]{:S(2)}, u32[]{:S(2)}) collective-permute-start(bf16[192,128]{1,0:T(8,128)(2,1)S(1)} %get-tuple-element.34), channel_id=1, source_target_pairs={{0,8},{4,12},{8,0},{12,4},{16,24},{20,28},{24,16},{28,20},{1,9},{5... | collective-permute-start | bytes 147464 | tf_op jit(solution)/shard_map/ppermute | solution.py:17
  56.6 1.5 %collective-permute-start.14 = (bf16[48,2048]{1,0:T(8,128)(2,1)S(1)}, bf16[48,2048]{1,0:T(8,128)(2,1)S(1)}, u32[]{:S(2)}, u32[]{:S(2)}) collective-permute-start(bf16[48,2048]{1,0:T(8,128)(2,1)S(1)} %get-tuple-element.40), channel_id=1, source_target_pairs={{0,1},{1,0},{2,3},{3,2},{4,5},{5,4},{6,7},{7,6},{8,9},{9,8},{10,11... | collective-permute-start | bytes 589832 | tf_op jit(solution)/shard_map/ppermute | solution.py:17
  56.7 3.1 %collective-permute-start.13 = (bf16[48,2048]{1,0:T(8,128)(2,1)S(1)}, bf16[48,2048]{1,0:T(8,128)(2,1)S(1)}, u32[]{:S(2)}, u32[]{:S(2)}) collective-permute-start(bf16[48,2048]{1,0:T(8,128)(2,1)S(1)} %get-tuple-element.38), channel_id=1, source_target_pairs={{0,1},{1,0},{2,3},{3,2},{4,5},{5,4},{6,7},{7,6},{8,9},{9,8},{10,11... | collective-permute-start | bytes 589832 | tf_op jit(solution)/shard_map/ppermute | solution.py:17
  58.1 7.0 %collective-permute-start.15 = (bf16[48,2048]{1,0:T(8,128)(2,1)S(1)}, bf16[48,2048]{1,0:T(8,128)(2,1)S(1)}, u32[]{:S(2)}, u32[]{:S(2)}) collective-permute-start(bf16[48,2048]{1,0:T(8,128)(2,1)S(1)} %add_convert_fusion.1), channel_id=1, source_target_pairs={{0,2},{1,3},{2,0},{3,1},{4,6},{5,7},{6,4},{7,5},{8,10},{9,11},{10,... | collective-permute-start | bytes 589832 | tf_op jit(solution)/shard_map/ppermute | solution.py:17
